TPU v7x, 32 devices: a whole 2x2x4 slice. The times are simulated.
32 devices in a mesh: sp: 16 (over z, x, core), tp: 2 (over y).
Axes of the slice: x: 2, y: 2, z: 4, core: 2. Of those that a mesh axis runs over, the one named last changes fastest.
Arguments:
- queries: bfloat16 [10240, 1024], P('sp', 'tp'), may hold values from -160 to 160
- keys: bfloat16 [10240, 256], P('sp', 'tp'), may hold values from -24 to 24
- values: bfloat16 [10240, 256], P('sp', 'tp'), may hold values from -6 to 6
- documents: int32 [10240], P('sp'), may hold values from 0 to 3, never falling along the last dimension, each value on 1 to 5120 neighbouring positions
- sinks: float32 [16], P('tp'), may hold values from -1 to 4
- out_weight: bfloat16 [1024, 2048], replicated, may hold values from -0.1875 to 0.1875
- residual: bfloat16 [10240, 2048], P(('sp', 'tp')), may hold values from -3 to 3
- norm_gain: float32 [2048], replicated, may hold values from 0.1 to 1.9
- up_weight: bfloat16 [2048, 8192], P('sp', 'tp'), may hold values from -0.125 to 0.125
- down_weight: bfloat16 [8192, 2048], P('tp', 'sp'), may hold values from -0.0625 to 0.0625
Outputs:
- layer_out: bfloat16 [10240, 2048], P(('sp', 'tp'))
Inputs may be any that keep to these rules, and one draw needn't show every extreme that they name: `documents`: document numbers never fall along the positions; each document holds at most 5120 positions.
All inputs are finite; a program needn't handle non-finite values.
Results may differ from a plain program's by a relative error of at most 0.0095.
Values may be sent and summed in bfloat16 or wider, within the bound.
A program may use at most 128 MiB of HBM per device.

v0:
```python
import jax
import jax.numpy as jnp
from jax import lax
from jax.sharding import PartitionSpec as P

HEAD_SIZE = 64
WINDOW_REACH = 128


masked_score = -1e30
epsilon = 1e-06


def passed_along(shard, axis, by):
    peers = lax.axis_size(axis)
    pairs = [(i, i + by) for i in range(peers) if 0 <= i + by < peers]
    return lax.ppermute(shard, axis, pairs)


def rounded(value):
    return lax.optimization_barrier(value.astype(jnp.bfloat16))


def squared_relu(before):
    return jnp.square(jax.nn.relu(before)).astype(jnp.bfloat16)


def windowed_attention(queries, keys, values, documents, sinks):
    length = queries.shape[0]
    heads = queries.shape[1] // HEAD_SIZE
    kv_heads = keys.shape[1] // HEAD_SIZE
    query_group = heads // kv_heads
    block_list = length // WINDOW_REACH
    prev_keys, prev_values, prev_docs = passed_along(
        (
            keys[length - WINDOW_REACH :],
            values[length - WINDOW_REACH :],
            documents[length - WINDOW_REACH :],
        ),
        "sp",
        1,
    )
    offset = lax.axis_index("sp") * length
    key_matrix = jnp.concatenate([prev_keys, keys], axis=0).reshape(
        block_list + 1, WINDOW_REACH, kv_heads, HEAD_SIZE
    )
    value_matrix = jnp.concatenate([prev_values, values], axis=0).reshape(
        block_list + 1, WINDOW_REACH, kv_heads, HEAD_SIZE
    )
    key_docs = jnp.concatenate([prev_docs, documents], axis=0).reshape(block_list + 1, WINDOW_REACH)
    key_place = (
        offset - WINDOW_REACH + jnp.arange((block_list + 1) * WINDOW_REACH, dtype=jnp.int32)
    ).reshape(block_list + 1, WINDOW_REACH)
    band_keys = jnp.concatenate([key_matrix[:-1], key_matrix[1:]], axis=1)
    band_values = jnp.concatenate([value_matrix[:-1], value_matrix[1:]], axis=1)
    band_docs = jnp.concatenate([key_docs[:-1], key_docs[1:]], axis=1)
    band_place = jnp.concatenate([key_place[:-1], key_place[1:]], axis=1)
    query_docs = documents.reshape(block_list, WINDOW_REACH)
    grouped_queries = queries.reshape(block_list, WINDOW_REACH, kv_heads, query_group, HEAD_SIZE)
    scores = jnp.einsum(
        "nqhgd,nshd->nhgqs", grouped_queries, band_keys, preferred_element_type=jnp.float32
    ) * HEAD_SIZE ** (-0.5)
    row_index = jnp.arange(WINDOW_REACH, dtype=jnp.int32)[:, None]
    col_index = jnp.arange(2 * WINDOW_REACH, dtype=jnp.int32)[None, :]
    distance = WINDOW_REACH + row_index - col_index
    near = (distance >= 0) & (distance < WINDOW_REACH)
    visible = (
        near[None]
        & (band_docs[:, None, :] == query_docs[:, :, None])
        & (band_place[:, None, :] >= 0)
    )
    visible = visible[:, None, None]
    head_sink_logit = sinks.reshape(kv_heads, query_group)[None, :, :, None]
    scores = jnp.where(visible, scores, masked_score)
    top = jnp.maximum(jnp.max(scores, axis=-1), head_sink_logit)
    exponent = jnp.where(visible, jnp.exp(scores - top[..., None]), 0.0)
    total = jnp.exp(head_sink_logit - top) + jnp.sum(exponent, axis=-1)
    shares = (exponent / total[..., None]).astype(jnp.bfloat16)
    attended = jnp.einsum(
        "nhgqs,nshd->nqhgd", shares, band_values, preferred_element_type=jnp.float32
    )
    return attended.astype(jnp.bfloat16).reshape(length, heads * HEAD_SIZE)


def rotated(shard, axis, by):
    peers = lax.axis_size(axis)
    return lax.ppermute(shard, axis, [(i, (i + by) % peers) for i in range(peers)])


def row_block(array, index, rows):
    return lax.dynamic_slice_in_dim(array, index * rows, rows, axis=0)


def body(
    queries, keys, values, documents, sinks, out_weight, residual, norm_gain, up_weight, down_weight
):
    up_whole, down_whole = (
        lax.all_gather(up_weight, "sp", axis=0, tiled=True),
        lax.all_gather(down_weight, "sp", axis=1, tiled=True),
    )
    n_tp = lax.axis_size("tp")
    me = lax.axis_index("tp")
    rows = residual.shape[0]
    attended = windowed_attention(queries, keys, values, documents, sinks)
    width = attended.shape[1]
    token_heads = jnp.zeros((rows, width * n_tp), jnp.bfloat16)
    for by in range(n_tp):
        piece = row_block(attended, (me + by) % n_tp, rows)
        if by:
            piece = rotated(piece, "tp", by)
        token_heads = lax.dynamic_update_slice_in_dim(
            token_heads, piece, ((me - by) % n_tp) * width, axis=1
        )
    projected = jnp.dot(token_heads, out_weight, preferred_element_type=jnp.float32)
    mixed = rounded(residual.astype(jnp.float32) + rounded(projected).astype(jnp.float32))
    widened = mixed.astype(jnp.float32)
    normed = (
        widened
        * lax.rsqrt(jnp.mean(widened * widened, axis=-1, keepdims=True) + epsilon)
        * norm_gain
    ).astype(jnp.bfloat16)
    branch = 0.0
    for by in range(n_tp - 1, -1, -1):
        rows_in = rotated(normed, "tp", by) if by else normed
        hidden = squared_relu(jnp.dot(rows_in, up_whole, preferred_element_type=jnp.float32))
        partial = jnp.dot(hidden, down_whole, preferred_element_type=jnp.float32).astype(
            jnp.bfloat16
        )
        if by:
            partial = rotated(partial, "tp", n_tp - by)
        branch = branch + partial.astype(jnp.float32)
    return (widened + rounded(branch).astype(jnp.float32)).astype(jnp.bfloat16)


def solution(mesh):
    in_specs = (
        P("sp", "tp"),
        P("sp", "tp"),
        P("sp", "tp"),
        P("sp"),
        P("tp"),
        P(),
        P(("sp", "tp"), None),
        P(),
        P("sp", "tp"),
        P("tp", "sp"),
    )
    out_specs = P(("sp", "tp"), None)
    return jax.shard_map(body, mesh=mesh, in_specs=in_specs, out_specs=out_specs, check_vma=False)
```

profile of v0, /device:TPU:0, one launch (start us, length us, event | category | flops | bytes accessed | tf_op | source)
XLA Modules:
  0.0 333.4 jit_solution(15821714109636754453)
XLA Ops:
  6.5 0.0 all-gather.3.cloned.1.call-start
  6.5 0.7 all-gather.3.cloned.1.call-update
  7.3 0.0 copy-start.7
  7.3 0.0 copy-start.5
  7.3 0.0 copy-start.2
  7.3 0.0 all-gather.5.cloned.1.call-start
  7.3 0.7 all-gather.5.cloned.1.call-update
  8.0 0.7 slice.63
  8.7 2.4 collective-permute-start.1
  11.1 0.8 slice.69
  11.9 4.5 %collective-permute-start.2 = (bf16[128,128]{1,0:T(8,128)(2,1)S(1)}, bf16[128,128]{1,0:T(8,128)(2,1)S(1)}, u32[]{:S(2)}, u32[]{:S(2)}) collective-permute-start(bf16[128,128]{1,0:T(8,128)(2,1)S(1)} %slice.69), channel_id=1, source_target_pairs={{0,2},{2,4},{4,6},{6,8},{8,10},{10,12},{12,14},{14,16},{16,18},{18... | collective-permute-start | bytes 98312 | tf_op jit(solution)/shard_map/ppermute | solution.py:17
  16.4 0.8 slice.59
  17.1 1.9 collective-permute-start
  19.1 1.1 reshape.107
  20.2 0.0 copy-done.3
  20.2 0.2 reshape.105
  20.5 0.0 copy-done.4
  20.5 0.7 reshape.108
  21.2 0.2 copy.20
  21.4 0.0 copy-done.7
  21.4 0.1 max.29
  21.5 0.2 copy.16
  21.7 0.0 collective-permute-done.1
  21.7 0.0 copy-done.5
  21.7 0.5 and_and_fusion
  22.2 0.0 collective-permute-done.2
  22.3 0.0 copy-done.2
  22.3 0.2 reshape.106
  22.4 0.2 copy.19
  22.6 0.0 collective-permute-done
  22.7 0.2 reshape.104
  22.8 0.2 copy.15
  23.0 1.1 fusion.6
  24.1 0.1 broadcast_maximum_fusion
  24.2 1.4 fusion.7
  25.6 0.1 exponential_add_fusion
  25.7 1.6 fusion.21
  27.3 0.5 copy.24
  27.8 0.1 copy.44
  27.9 0.1 broadcast_in_dim.31
  28.0 0.4 constant_dynamic-slice_fusion
  28.4 1.6 collective-permute-start.3
  30.0 9.8 %collective-permute-done.3 = bf16[320,512]{0,1:T(8,128)(2,1)S(1)} collective-permute-done((bf16[320,512]{0,1:T(8,128)(2,1)S(1)}, bf16[320,512]{0,1:T(8,128)(2,1)S(1)}, u32[]{:S(2)}, u32[]{:S(2)}) %collective-permute-start.3) | collective-permute-done | bytes 327712 | tf_op jit(solution)/shard_map/ppermute | solution.py:87
  39.7 0.1 constant_dynamic-update-slice_fusion
  39.8 0.0 copy-start.1
  39.8 3.9 %convolution_convert_fusion = bf16[320,2048]{1,0:T(8,128)(2,1)S(1)} fusion(bf16[320,1024]{0,1:T(8,128)(2,1)S(1)} %constant_dynamic-update-slice_fusion, bf16[1024,2048]{1,0:T(8,128)(2,1)} %param.15), kind=kOutput, calls=%fused_computation.19 | convolution fusion | flops 1342832640 | bytes 6160384 | tf_op jit(solution)/shard_map/dot_general | solution.py:114
  43.7 0.0 copy-done.1
  43.7 0.0 copy-start.6
  43.7 0.5 add_convert_fusion.1
  44.2 0.4 fusion.11
  44.6 0.0 copy-done.6
  44.6 0.4 fusion.13
  44.9 0.0 copy-start
  45.0 1.0 copy-done
  46.0 1.5 collective-permute-start.4
  47.5 30.0 %collective-permute-done.4 = bf16[320,2048]{1,0:T(8,128)(2,1)S(1)} collective-permute-done((bf16[320,2048]{1,0:T(8,128)(2,1)S(1)}, bf16[320,2048]{1,0:T(8,128)(2,1)S(1)}, u32[]{:S(2)}, u32[]{:S(2)}) %collective-permute-start.4) | collective-permute-done | bytes 1310752 | tf_op jit(solution)/shard_map/ppermute | solution.py:87
  77.6 61.2 %all-gather.3.cloned.1.call-done = bf16[2048,4096]{1,0:T(8,128)(2,1)} async-done(((bf16[128,4096]{1,0:T(8,128)(2,1)}), bf16[2048,4096]{1,0:T(8,128)(2,1)}) %all-gather.3.cloned.1.call-update) | async-done | bytes 16777232 | tf_op jit(solution)/shard_map/all_gather | solution.py:98
  138.7 130.2 %all-gather.5.cloned.1.call-done = bf16[4096,2048]{1,0:T(8,128)(2,1)} async-done(((bf16[4096,128]{1,0:T(8,128)(2,1)}), bf16[4096,2048]{1,0:T(8,128)(2,1)}) %all-gather.5.cloned.1.call-update) | async-done | bytes 16777232 | tf_op jit(solution)/shard_map/all_gather | solution.py:99
  269.0 22.8 %fusion.10 = bf16[320,2048]{1,0:T(8,128)(2,1)} fusion(bf16[4096,2048]{1,0:T(8,128)(2,1)} %all-gather.5.cloned.1.call-done, bf16[320,2048]{1,0:T(8,128)(2,1)S(1)} %collective-permute-done.4, bf16[2048,4096]{1,0:T(8,128)(2,1)} %all-gather.3.cloned.1.call-done), kind=kOutput, calls=%fused_computation.18 | convolution fusion | flops 10742005760 | bytes 36175872 | tf_op jit(solution)/shard_map/dot_general | solution.py:126
  291.8 1.5 collective-permute-start.5
  293.2 23.4 %fusion.9 = f32[320,2048]{1,0:T(8,128)} fusion(bf16[4096,2048]{1,0:T(8,128)(2,1)} %all-gather.5.cloned.1.call-done, bf16[320,2048]{1,0:T(8,128)(2,1)} %copy-done, bf16[2048,4096]{1,0:T(8,128)(2,1)} %all-gather.3.cloned.1.call-done), kind=kOutput, calls=%fused_computation.17 | convolution fusion | flops 10742661120 | bytes 37486592 | tf_op jit(solution)/shard_map/dot_general | solution.py:126
  316.6 6.3 %collective-permute-done.5 = bf16[320,2048]{1,0:T(8,128)(2,1)S(1)} collective-permute-done((bf16[320,2048]{1,0:T(8,128)(2,1)}, bf16[320,2048]{1,0:T(8,128)(2,1)S(1)}, u32[]{:S(2)}, u32[]{:S(2)}) %collective-permute-start.5) | collective-permute-done | bytes 1310752 | tf_op jit(solution)/shard_map/ppermute | solution.py:87
  322.9 2.2 add_convert_fusion
  325.1 1.5 fusion.14
  (13 shorter events, 0.1 us)
Async XLA Ops:
  6.5 13.7 %copy-start.3 = (bf16[640,128]{1,0:T(8,128)(2,1)S(1)}, bf16[640,128]{1,0:T(8,128)(2,1)}, u32[]{:S(2)}) copy-start(bf16[640,128]{1,0:T(8,128)(2,1)} %param.12) | copy-start | bytes 491524
  6.5 13.9 %copy-start.4 = (bf16[640,512]{1,0:T(8,128)(2,1)S(1)}, bf16[640,512]{1,0:T(8,128)(2,1)}, u32[]{:S(2)}) copy-start(bf16[640,512]{1,0:T(8,128)(2,1)} %param.10) | copy-start | bytes 1966084
  6.5 132.2 %all-gather.3.cloned.1.call-start = ((), (), s32[]{:S(2)}) async-start(), calls=%async_computation | async-start | bytes 17825792 | tf_op jit(solution)/shard_map/all_gather | solution.py:98
  7.3 14.1 %copy-start.7 = (f32[8]{0:T(128)S(1)}, f32[8]{0:T(128)}, u32[]{:S(2)}) copy-start(f32[8]{0:T(128)} %param.14) | copy-start | bytes 100
  7.3 14.4 %copy-start.5 = (s32[640]{0:T(1024)S(1)}, s32[640]{0:T(1024)}, u32[]{:S(2)}) copy-start(s32[640]{0:T(1024)} %param.13) | copy-start | bytes 7684
  7.3 15.0 %copy-start.2 = (bf16[640,128]{1,0:T(8,128)(2,1)S(1)}, bf16[640,128]{1,0:T(8,128)(2,1)}, u32[]{:S(2)}) copy-start(bf16[640,128]{1,0:T(8,128)(2,1)} %param.11) | copy-start | bytes 491524
  7.3 261.7 %all-gather.5.cloned.1.call-start = ((), (), s32[]{:S(2)}) async-start(), calls=%async_computation.1 | async-start | bytes 17825792 | tf_op jit(solution)/shard_map/all_gather | solution.py:99
  8.7 12.9 %collective-permute-start.1 = (s32[128]{0:T(128)S(1)}, s32[128]{0:T(128)S(1)}, u32[]{:S(2)}, u32[]{:S(2)}) collective-permute-start(s32[128]{0:T(128)S(1)} %slice.63), channel_id=1, source_target_pairs={{0,2},{2,4},{4,6},{6,8},{8,10},{10,12},{12,14},{14,16},{16,18},{18... | collective-permute-start | bytes 1544 | tf_op jit(solution)/shard_map/ppermute | solution.py:17
  11.9 10.4 %collective-permute-start.2 = (bf16[128,128]{1,0:T(8,128)(2,1)S(1)}, bf16[128,128]{1,0:T(8,128)(2,1)S(1)}, u32[]{:S(2)}, u32[]{:S(2)}) collective-permute-start(bf16[128,128]{1,0:T(8,128)(2,1)S(1)} %slice.69), channel_id=1, source_target_pairs={{0,2},{2,4},{4,6},{6,8},{8,10},{10,12},{12,14},{14,16},{16,18},{18... | collective-permute-start | bytes 98312 | tf_op jit(solution)/shard_map/ppermute | solution.py:17
  17.1 5.5 %collective-permute-start = (bf16[128,128]{1,0:T(8,128)(2,1)S(1)}, bf16[128,128]{1,0:T(8,128)(2,1)S(1)}, u32[]{:S(2)}, u32[]{:S(2)}) collective-permute-start(bf16[128,128]{1,0:T(8,128)(2,1)S(1)} %slice.59), channel_id=1, source_target_pairs={{0,2},{2,4},{4,6},{6,8},{8,10},{10,12},{12,14},{14,16},{16,18},{18... | collective-permute-start | bytes 98312 | tf_op jit(solution)/shard_map/ppermute | solution.py:17
  28.4 11.4 %collective-permute-start.3 = (bf16[320,512]{0,1:T(8,128)(2,1)S(1)}, bf16[320,512]{0,1:T(8,128)(2,1)S(1)}, u32[]{:S(2)}, u32[]{:S(2)}) collective-permute-start(bf16[320,512]{0,1:T(8,128)(2,1)S(1)} %get-tuple-element.5), channel_id=1, source_target_pairs={{0,1},{1,0},{2,3},{3,2},{4,5},{5,4},{6,7},{7,6},{8,9},{9,8},{10,11... | collective-permute-start | bytes 983048 | tf_op jit(solution)/shard_map/ppermute | solution.py:87
  39.8 3.9 %copy-start.1 = (bf16[320,2048]{1,0:T(8,128)(2,1)S(1)}, bf16[320,2048]{1,0:T(8,128)(2,1)}, u32[]{:S(2)}) copy-start(bf16[320,2048]{1,0:T(8,128)(2,1)} %param.16) | copy-start | bytes 3932164
  43.7 0.9 copy-start.6
  44.9 1.1 copy-start
  46.0 31.5 %collective-permute-start.4 = (bf16[320,2048]{1,0:T(8,128)(2,1)S(1)}, bf16[320,2048]{1,0:T(8,128)(2,1)S(1)}, u32[]{:S(2)}, u32[]{:S(2)}) collective-permute-start(bf16[320,2048]{1,0:T(8,128)(2,1)S(1)} %fusion.13), channel_id=1, source_target_pairs={{0,1},{1,0},{2,3},{3,2},{4,5},{5,4},{6,7},{7,6},{8,9},{9,8},{10,11... | collective-permute-start | bytes 3932168 | tf_op jit(solution)/shard_map/ppermute | solution.py:87
  291.8 31.1 %collective-permute-start.5 = (bf16[320,2048]{1,0:T(8,128)(2,1)}, bf16[320,2048]{1,0:T(8,128)(2,1)S(1)}, u32[]{:S(2)}, u32[]{:S(2)}) collective-permute-start(bf16[320,2048]{1,0:T(8,128)(2,1)} %fusion.10), channel_id=1, source_target_pairs={{0,1},{1,0},{2,3},{3,2},{4,5},{5,4},{6,7},{7,6},{8,9},{9,8},{10,11... | collective-permute-start | bytes 3932168 | tf_op jit(solution)/shard_map/ppermute | solution.py:87
Sparse Core Ops, SparseCore 0:
  9.5 129.1 all-gather.2
  140.9 128.0 all-gather.4
where the time goes:
time: 334 us; the launch traced here: 333 us
  waiting for transfers between devices  239 us (72%)
  matrix products  52.7 us (16%)
  between operations  13.8 us (4%)
  starting transfers between devices  13.4 us (4%)
  local copies, waits for them, and re-layouts  7.48 us (2%)
  other arithmetic  7.12 us (2%)
    all_gather x1, waiting for transfers between devices, body(): lax.all_gather(down_weight, 'sp', axis=1, tiled=True)  130 us
    all_gather x1, waiting for transfers between devices, body(): lax.all_gather(up_weight, 'sp', axis=0, tiled=True)  61.2 us
    dot_general x2, matrix products, body(): jnp.dot(hidden, down_whole, preferred_element_type=jnp.float32)  46.2 us
    ppermute x3, waiting for transfers between devices, rotated(): lax.ppermute(shard, axis, [(i, (i + by) % peers) for i in range(peers)])  46.1 us
    ppermute x3, starting transfers between devices, passed_along(): return lax.ppermute(shard, axis, pairs)  8.78 us
  transfers between devices with their start and end apart: 8, of which 5 were waited for; matrix products, arithmetic and copies ran while one was open for 12% of the time, Pallas kernels for 0%

commit v1 on v0

--- a/solution.py
+++ b/solution.py
@@ -1,11 +1,17 @@
+import functools
+
 import jax
 import jax.numpy as jnp
 from jax import lax
+from jax.experimental import pallas as pl
+from jax.experimental.pallas import tpu as pltpu
 from jax.sharding import PartitionSpec as P
 
 HEAD_SIZE = 64
 WINDOW_REACH = 128
-
+LANES = 128
+CORES = 2
+MESH = pl.DeviceIdType.MESH
 
 masked_score = -1e30
 epsilon = 1e-06
@@ -91,7 +97,7 @@
     return lax.dynamic_slice_in_dim(array, index * rows, rows, axis=0)
 
 
-def body(
+def gathered_body(
     queries, keys, values, documents, sinks, out_weight, residual, norm_gain, up_weight, down_weight
 ):
     up_whole, down_whole = (
@@ -132,6 +138,472 @@
     return (widened + rounded(branch).astype(jnp.float32)).astype(jnp.bfloat16)
 
 
+def fits(mesh, tokens, width, kv_width, model, hidden):
+    n_sp, n_tp = mesh.shape["sp"], mesh.shape["tp"]
+    block = model // n_sp
+    return (
+        n_tp == 2
+        and n_sp % (n_tp * CORES) == 0
+        and block % LANES == 0
+        and kv_width == LANES
+        and width % (2 * LANES) == 0
+        and tokens % (2 * WINDOW_REACH // 2) == 0
+        and (tokens // n_tp) % 32 == 0
+        and hidden % (n_tp * 2 * LANES) == 0
+    )
+
+
+def layer_kernel(
+    n_z,
+    q_hbm, k_hbm, v_hbm, docs_hbm, sinks, outw_hbm, res_hbm, gain_ref, up_hbm, down_hbm,
+    out_hbm,
+    up_all, down_all, rows_all, hid_all, outw, res, mixed, q_ref, k_ref, v_ref, docs,
+    k_wide, v_wide, att, oth, psend, precv, own_sum, out_ref,
+    load_sem, halo_send, halo_recv, xs_sem, z_send, z_recv, d_send, d_recv, y_sem,
+    g_send, g_recv, p_send, p_recv, own_sem,
+):
+    sp, y = lax.axis_index("sp"), lax.axis_index("tp")
+    n_x, n_y = 2, 2
+    z, x, c = sp // (n_x * CORES), lax.rem(sp // CORES, n_x), lax.rem(sp, CORES)
+    n_sp = n_z * n_x * CORES
+    tokens = q_ref.shape[0]
+    rows = res.shape[0]
+    half = rows // 2
+    model = res.shape[1]
+    width = q_ref.shape[1]
+    blk = up_hbm.shape[0]
+    quarter = up_hbm.shape[1] // n_x
+    wide = 2 * blk
+
+    def at(zz, xx, yy, cc):
+        return ((zz * n_x + xx) * CORES + cc, yy)
+
+    def remote(src, dst, send, recv, dev):
+        return pltpu.make_async_remote_copy(
+            src_ref=src, dst_ref=dst, send_sem=send, recv_sem=recv, device_id=dev, device_id_type=MESH
+        )
+
+    x_peer, y_peer, c_peer = at(z, 1 - x, y, c), at(z, x, 1 - y, c), at(z, x, y, 1 - c)
+
+    def block(phase, zb, xb, cb):
+        if phase == 0:
+            first = ((zb * n_x + xb) * CORES + cb) * blk
+            return up_all.at[pl.ds(pl.multiple_of(first, blk), blk), :]
+        return down_all.at[zb * n_x + xb, :, pl.ds(pl.multiple_of(cb * blk, blk), blk)]
+
+    def own_piece(phase, xq):
+        start = pl.multiple_of(xq * quarter, quarter)
+        if phase == 0:
+            return up_hbm.at[:, pl.ds(start, quarter)]
+        return down_hbm.at[pl.ds(start, quarter), :]
+
+    def x_exchange(phase):
+        return remote(
+            own_piece(phase, 1 - x), block(phase, z, x, c), xs_sem.at[phase], z_recv.at[phase, z, 1], x_peer
+        )
+
+    def own_load(phase):
+        return pltpu.make_async_copy(own_piece(phase, x), block(phase, z, x, c), own_sem.at[phase])
+
+    low = jnp.minimum(z, n_z - 1 - z)
+
+    def plane(k):
+        near = jnp.where(lax.rem(k, 2) == 1, z - (k + 1) // 2, z + (k + 1) // 2)
+        far = jnp.where(z < n_z - 1 - z, k, n_z - 1 - k)
+        return jnp.where(k <= 2 * low, near, far)
+
+    def place(t):
+        zb, b = plane(t // 2), lax.rem(t, 2)
+        return zb, b, jnp.where(b == 0, x, 1 - x)
+
+    def to_up(phase, zb, b, xb):
+        ref = block(phase, zb, xb, c)
+        return remote(ref, ref, z_send.at[0, phase, zb, b], z_recv.at[phase, zb, b], at(z + 1, x, y, c))
+
+    def to_down(phase, zb, b, xb):
+        ref = block(phase, zb, xb, c)
+        return remote(ref, ref, z_send.at[1, phase, zb, b], z_recv.at[phase, zb, b], at(z - 1, x, y, c))
+
+    def to_core(phase, zb, b, xb):
+        ref = block(phase, zb, xb, c)
+        return remote(ref, ref, d_send.at[phase, zb, b], d_recv.at[phase, zb, b], c_peer)
+
+    def goes_up(zb):
+        return jnp.logical_and(zb <= z, z < n_z - 1)
+
+    def goes_down(zb):
+        return jnp.logical_and(zb >= z, z > 0)
+
+    def pass_on(phase, t):
+        zb, b, xb = place(t)
+
+        @pl.when(goes_up(zb))
+        def _():
+            to_up(phase, zb, b, xb).start()
+
+        @pl.when(goes_down(zb))
+        def _():
+            to_down(phase, zb, b, xb).start()
+
+        to_core(phase, zb, b, xb).start()
+
+    def arrive(phase, t):
+        zb, b, xb = place(t)
+        to_up(phase, zb, b, xb).wait_recv()
+        pass_on(phase, t)
+
+    last = tokens - WINDOW_REACH
+    nxt = (sp + 1, y)
+
+    def halo(i):
+        src, dst = (
+            (k_hbm.at[pl.ds(last, WINDOW_REACH), :], k_ref.at[pl.ds(0, WINDOW_REACH), :]),
+            (v_hbm.at[pl.ds(last, WINDOW_REACH), :], v_ref.at[pl.ds(0, WINDOW_REACH), :]),
+            (docs_hbm.at[last // LANES], docs.at[0]),
+        )[i]
+        return remote(src, dst, halo_send.at[i], halo_recv.at[i], nxt)
+
+    @pl.when(sp < n_sp - 1)
+    def _():
+        for i in range(3):
+            halo(i).start()
+
+    own_load(0).start()
+    loads = [
+        pltpu.make_async_copy(q_hbm, q_ref, load_sem.at[0]),
+        pltpu.make_async_copy(k_hbm, k_ref.at[pl.ds(WINDOW_REACH, tokens), :], load_sem.at[1]),
+        pltpu.make_async_copy(v_hbm, v_ref.at[pl.ds(WINDOW_REACH, tokens), :], load_sem.at[2]),
+        pltpu.make_async_copy(docs_hbm, docs.at[pl.ds(1, tokens // LANES)], load_sem.at[3]),
+        pltpu.make_async_copy(outw_hbm, outw, load_sem.at[4]),
+        pltpu.make_async_copy(res_hbm, res, load_sem.at[5]),
+    ]
+    x_exchange(0).start()
+    own_load(0).wait()
+    pass_on(0, 0)
+    for load in loads:
+        load.start()
+    own_load(1).start()
+    x_exchange(1).start()
+
+    @pl.when(sp == 0)
+    def _():
+        k_ref[pl.ds(0, WINDOW_REACH), :] = jnp.zeros((WINDOW_REACH, LANES), jnp.bfloat16)
+        v_ref[pl.ds(0, WINDOW_REACH), :] = jnp.zeros((WINDOW_REACH, LANES), jnp.bfloat16)
+        docs[0] = jnp.full(docs.shape[1:], -1, jnp.int32)
+
+    for load in loads[:4]:
+        load.wait()
+
+    @pl.when(sp > 0)
+    def _():
+        for i in range(3):
+            halo(i).wait_recv()
+
+    heads = width // HEAD_SIZE
+    kv_heads = LANES // HEAD_SIZE
+    group = heads // kv_heads
+    lane_in = lax.broadcasted_iota(jnp.int32, (LANES, LANES), 0)
+    lane_out = lax.broadcasted_iota(jnp.int32, (LANES, LANES), 1)
+    for g in range(kv_heads):
+        for par in range(2):
+            pick = (lane_in - g * HEAD_SIZE == lane_out - par * HEAD_SIZE) & (
+                lane_out // HEAD_SIZE == par
+            )
+            pick = pick.astype(jnp.float32).astype(jnp.bfloat16)
+            for raw, spread in ((k_ref, k_wide), (v_ref, v_wide)):
+                spread[g * 2 + par] = jnp.dot(
+                    raw[...], pick, preferred_element_type=jnp.float32
+                ).astype(jnp.bfloat16)
+
+    row_i = lax.broadcasted_iota(jnp.int32, (WINDOW_REACH, 2 * WINDOW_REACH), 0)
+    col_i = lax.broadcasted_iota(jnp.int32, (WINDOW_REACH, 2 * WINDOW_REACH), 1)
+    near = (col_i > row_i) & (col_i <= row_i + WINDOW_REACH)
+
+    def attend(n, carry):
+        start = pl.multiple_of(n * WINDOW_REACH, WINDOW_REACH)
+        early = jnp.broadcast_to(docs[n], (WINDOW_REACH, LANES))
+        late = jnp.broadcast_to(docs[n + 1], (WINDOW_REACH, LANES))
+        mine = late.T
+        same = jnp.concatenate([early == mine, late == mine], axis=1)
+        visible = near & same
+        for j in range(width // LANES):
+            total_out = None
+            g = (2 * j) // group
+            q_blk = q_ref[pl.ds(start, WINDOW_REACH), j * LANES : (j + 1) * LANES]
+            for par in range(2):
+                head = 2 * j + par
+                keys = k_wide[g * 2 + par, pl.ds(start, 2 * WINDOW_REACH), :]
+                vals = v_wide[g * 2 + par, pl.ds(start, 2 * WINDOW_REACH), :]
+                scores = lax.dot_general(
+                    q_blk, keys, (((1,), (1,)), ((), ())), preferred_element_type=jnp.float32
+                ) * HEAD_SIZE ** (-0.5)
+                scores = jnp.where(visible, scores, masked_score)
+                sink = sinks[head]
+                top = jnp.maximum(jnp.max(scores, axis=1, keepdims=True), sink)
+                exponent = jnp.where(visible, jnp.exp(scores - top), 0.0)
+                total = jnp.exp(sink - top) + jnp.sum(exponent, axis=1, keepdims=True)
+                shares = (exponent * (1.0 / total)).astype(jnp.bfloat16)
+                part = jnp.dot(shares, vals, preferred_element_type=jnp.float32)
+                total_out = part if total_out is None else total_out + part
+            att[pl.ds(start, WINDOW_REACH), j * LANES : (j + 1) * LANES] = total_out.astype(
+                jnp.bfloat16
+            )
+        return carry
+
+    lax.fori_loop(0, tokens // WINDOW_REACH, attend, 0)
+
+    mine_at = pl.multiple_of(y * rows, rows)
+    theirs_at = pl.multiple_of((1 - y) * rows, rows)
+    swap = remote(att.at[pl.ds(theirs_at, rows), :], oth, y_sem.at[0], y_sem.at[1], y_peer)
+    swap.start()
+    arrive(0, 1)
+    arrive(0, 2)
+    loads[4].wait()
+    loads[5].wait()
+    swap.wait_recv()
+
+    me_p = x * n_y + y
+    x_p, y_p, d_p = (1 - x) * n_y + y, x * n_y + 1 - y, (1 - x) * n_y + 1 - y
+    chunk = 2 * wide
+
+    def row_part(p, h):
+        return rows_all.at[pl.ds(pl.multiple_of(p * rows + h * half, half), half), :]
+
+    def give(p, h, way):
+        slot = p * 2 + h
+        ref = row_part(p, h)
+        return remote(ref, ref, g_send.at[way, slot], g_recv.at[slot], x_peer if way == 0 else y_peer)
+
+    for h in range(2):
+        own_rows = pl.ds(pl.multiple_of(mine_at + h * half, half), half)
+
+        def project(n, square):
+            cols = pl.ds(pl.multiple_of(n * chunk, chunk), chunk)
+            acc = jnp.dot(
+                att[own_rows, :], outw[pl.ds(pl.multiple_of(y * width, width), width), cols],
+                preferred_element_type=jnp.float32,
+            ) + jnp.dot(
+                oth[h * half : (h + 1) * half, :],
+                outw[pl.ds(pl.multiple_of((1 - y) * width, width), width), cols],
+                preferred_element_type=jnp.float32,
+            )
+            sums = res[h * half : (h + 1) * half, cols].astype(jnp.float32) + acc.astype(
+                jnp.bfloat16
+            ).astype(jnp.float32)
+            sums = sums.astype(jnp.bfloat16)
+            mixed[h * half : (h + 1) * half, cols] = sums
+            sums = sums.astype(jnp.float32)
+            return square + jnp.sum(sums * sums, axis=1, keepdims=True)
+
+        square = lax.fori_loop(0, model // chunk, project, jnp.zeros((half, 1), jnp.float32))
+        scale = lax.rsqrt(square * (1.0 / model) + epsilon)
+
+        def normalise(n, carry):
+            cols = pl.ds(pl.multiple_of(n * chunk, chunk), chunk)
+            wide_rows = mixed[h * half : (h + 1) * half, cols].astype(jnp.float32)
+            rows_all[pl.ds(pl.multiple_of(me_p * rows + h * half, half), half), cols] = (
+                wide_rows * scale * gain_ref[:, cols]
+            ).astype(jnp.bfloat16)
+            return carry
+
+        lax.fori_loop(0, model // chunk, normalise, 0)
+        give(me_p, h, 0).start()
+        give(me_p, h, 1).start()
+
+    arrive(0, 3)
+    n_items = 2 * n_z
+
+    def more(first, until):
+        for t in range(first, min(until, n_items)):
+            arrive(0, t)
+
+    more(4, 6)
+    give(x_p, 0, 0).wait_recv()
+    give(x_p, 0, 1).start()
+    more(6, 7)
+    give(y_p, 1, 1).wait_recv()
+    give(y_p, 1, 0).start()
+    more(7, n_items)
+
+    own_load(1).wait()
+    pass_on(1, 0)
+    arrive(1, 1)
+
+    give(x_p, 1, 0).wait_recv()
+    give(y_p, 0, 1).wait_recv()
+    give(d_p, 0, 1).wait_recv()
+    give(d_p, 1, 0).wait_recv()
+
+    def core_wait(phase):
+        def wait_one(t, carry):
+            zb, b, xb = place(t)
+            to_core(phase, zb, b, xb).wait_recv()
+            return carry
+        return wait_one
+
+    lax.fori_loop(0, n_items, core_wait(0), 0)
+    tall = 2 * rows
+
+    def up_step(i, carry):
+        r = pl.ds(pl.multiple_of((i // (quarter // chunk)) * tall, tall), tall)
+        f = pl.ds(pl.multiple_of(lax.rem(i, quarter // chunk) * chunk, chunk), chunk)
+        before = jnp.dot(rows_all[r, :], up_all[:, f], preferred_element_type=jnp.float32)
+        before = jnp.maximum(before, 0.0)
+        hid_all[r, f] = (before * before).astype(jnp.bfloat16)
+        return carry
+
+    lax.fori_loop(0, 2 * (quarter // chunk), up_step, 0)
+
+    def partial_copy(j, s):
+        px, py = jnp.where(s >= 2, 1 - x, x), jnp.where(lax.rem(s, 2) == 1, 1 - y, y)
+        return remote(
+            psend.at[j, s - 1], precv.at[j, s - 1], p_send.at[j, s - 1], p_recv.at[j, s - 1], at(z, px, py, c)
+        )
+
+    def combine(t):
+        zb, b, xb = place(t)
+        j = zb * n_x + xb
+        total = own_sum[j]
+        for s in (1, 2, 3):
+            partial_copy(j, s).wait_recv()
+            total = total + precv[j, s - 1].astype(jnp.float32)
+        cols = pl.ds(pl.multiple_of(j * wide, wide), wide)
+        out_ref[:, cols] = (
+            mixed[:, cols].astype(jnp.float32) + total.astype(jnp.bfloat16).astype(jnp.float32)
+        ).astype(jnp.bfloat16)
+
+    def down_step(t, carry):
+        @pl.when(t >= 2)
+        def _():
+            arrive(1, t)
+
+        zb, b, xb = place(t)
+        to_core(1, zb, b, xb).wait_recv()
+        j = zb * n_x + xb
+
+        def piece(i, carry):
+            s = 3 - i
+            px, py = jnp.where(s >= 2, 1 - x, x), jnp.where(lax.rem(s, 2) == 1, 1 - y, y)
+            first = pl.multiple_of((px * n_y + py) * rows, rows)
+            part = jnp.dot(
+                hid_all[pl.ds(first, rows), :], down_all[j], preferred_element_type=jnp.float32
+            )
+
+            @pl.when(s > 0)
+            def _():
+                psend[j, s - 1] = part.astype(jnp.bfloat16)
+                partial_copy(j, s).start()
+
+            @pl.when(s == 0)
+            def _():
+                own_sum[j] = part
+
+            return carry
+
+        lax.fori_loop(0, n_x * n_y, piece, 0)
+
+        @pl.when(t >= 2)
+        def _():
+            combine(t - 2)
+
+        return carry
+
+    lax.fori_loop(0, n_items, down_step, 0)
+    for t in (n_items - 2, n_items - 1):
+        combine(jnp.int32(t))
+    store = pltpu.make_async_copy(out_ref, out_hbm, load_sem.at[0])
+    store.start()
+
+    @pl.when(sp < n_sp - 1)
+    def _():
+        for i in range(3):
+            halo(i).wait_send()
+
+    swap.wait_send()
+    for phase in range(2):
+        x_exchange(phase).wait_send()
+    for h in range(2):
+        give(me_p, h, 0).wait_send()
+        give(me_p, h, 1).wait_send()
+    give(x_p, 0, 1).wait_send()
+    give(y_p, 1, 0).wait_send()
+
+    def sent(t, carry):
+        zb, b, xb = place(t)
+        for phase in range(2):
+            @pl.when(goes_up(zb))
+            def _():
+                to_up(phase, zb, b, xb).wait_send()
+
+            @pl.when(goes_down(zb))
+            def _():
+                to_down(phase, zb, b, xb).wait_send()
+
+            to_core(phase, zb, b, xb).wait_send()
+        for s in (1, 2, 3):
+            partial_copy(zb * n_x + xb, s).wait_send()
+        return carry
+
+    lax.fori_loop(0, n_items, sent, 0)
+    store.wait()
+
+
+def kernel_body(
+    n_z, queries, keys, values, documents, sinks, out_weight, residual, norm_gain, up_weight, down_weight
+):
+    tokens, width = queries.shape
+    rows, model = residual.shape
+    blk, hidden = up_weight.shape
+    quarter = hidden // 2
+    group = 4 * rows
+    pairs = 2 * n_z
+    bf16, f32 = jnp.bfloat16, jnp.float32
+    hbm = pl.BlockSpec(memory_space=pl.ANY)
+    dma = pltpu.SemaphoreType.DMA
+    return pl.pallas_call(
+        functools.partial(layer_kernel, n_z),
+        out_shape=jax.ShapeDtypeStruct((rows, model), bf16),
+        in_specs=[hbm, hbm, hbm, hbm, pl.BlockSpec(memory_space=pltpu.SMEM), hbm, hbm,
+                  pl.BlockSpec(memory_space=pltpu.VMEM), hbm, hbm],
+        out_specs=hbm,
+        scratch_shapes=[
+            pltpu.VMEM((model, quarter), bf16),
+            pltpu.VMEM((pairs, quarter, 2 * blk), bf16),
+            pltpu.VMEM((group, model), bf16),
+            pltpu.VMEM((group, quarter), bf16),
+            pltpu.VMEM(out_weight.shape, bf16),
+            pltpu.VMEM((rows, model), bf16),
+            pltpu.VMEM((rows, model), bf16),
+            pltpu.VMEM((tokens, width), bf16),
+            pltpu.VMEM((tokens + WINDOW_REACH, LANES), bf16),
+            pltpu.VMEM((tokens + WINDOW_REACH, LANES), bf16),
+            pltpu.VMEM((tokens // LANES + 1, 1, LANES), jnp.int32),
+            pltpu.VMEM((4, tokens + WINDOW_REACH, LANES), bf16),
+            pltpu.VMEM((4, tokens + WINDOW_REACH, LANES), bf16),
+            pltpu.VMEM((tokens, width), bf16),
+            pltpu.VMEM((rows, width), bf16),
+            pltpu.VMEM((pairs, 3, rows, 2 * blk), bf16),
+            pltpu.VMEM((pairs, 3, rows, 2 * blk), bf16),
+            pltpu.VMEM((pairs, rows, 2 * blk), f32),
+            pltpu.VMEM((rows, model), bf16),
+            dma((6,)), dma((3,)), dma((3,)), dma((2,)), dma((2, 2, n_z, 2)), dma((2, n_z, 2)),
+            dma((2, n_z, 2)), dma((2, n_z, 2)), dma((2,)), dma((2, 8)), dma((8,)),
+            dma((pairs, 3)), dma((pairs, 3)), dma((2,)),
+        ],
+        compiler_params=pltpu.CompilerParams(has_side_effects=True, vmem_limit_bytes=67043328),
+    )(
+        queries, keys, values, documents.reshape(tokens // LANES, 1, LANES), sinks, out_weight,
+        residual, norm_gain.reshape(1, model), up_weight, down_weight,
+    )
+
+
+def body(n_z, mesh, *arrays):
+    queries, keys, up_weight, residual = arrays[0], arrays[1], arrays[8], arrays[6]
+    if fits(mesh, *queries.shape, keys.shape[1], residual.shape[1], up_weight.shape[1]):
+        return kernel_body(n_z, *arrays)
+    return gathered_body(*arrays)
+
+
 def solution(mesh):
     in_specs = (
         P("sp", "tp"),
@@ -146,4 +618,7 @@
         P("tp", "sp"),
     )
     out_specs = P(("sp", "tp"), None)
-    return jax.shard_map(body, mesh=mesh, in_specs=in_specs, out_specs=out_specs, check_vma=False)
+    n_z = mesh.shape["sp"] // (CORES * mesh.shape["tp"])
+    return jax.shard_map(
+        functools.partial(body, n_z, mesh), mesh=mesh, in_specs=in_specs, out_specs=out_specs, check_vma=False
+    )

time: 334 us -> 174 us (0.52)
  waiting for transfers between devices: 239 us -> 0 us
  Pallas kernels: 0 us -> 170 us
  matrix products: 52.7 us -> 0 us
  between operations: 13.8 us -> 0.01 us
  starting transfers between devices: 13.4 us -> 0 us
  other arithmetic: 7.12 us -> 0 us
  local copies, waits for them, and re-layouts: 7.48 us -> 3.79 us
    all_gather x2 -> x0, waiting for transfers between devices: 191 us -> none  [the longest x1 130 us: body(): lax.all_gather(down_weight, 'sp', axis=1, tiled=True)]
    pallas_call x0 -> x1, Pallas kernels: none -> 170 us  [kernel_body(): pl.pallas_call(functools.partial(layer_kernel, n_z), out_shape=jax.ShapeD...]
    dot_general x5 -> x0, matrix products: 52.7 us -> none  [the longest x2 46.2 us: body(): jnp.dot(hidden, down_whole, preferred_element_type=jnp.float32)]
    ppermute x6 -> x0, waiting for transfers between devices: 46.1 us -> none  [the longest x3 46.1 us: rotated(): lax.ppermute(shard, axis, [(i, (i + by) % peers) for i in range(peers)])]
    ppermute x6 -> x0, starting transfers between devices: 13.4 us -> none  [the longest x3 8.78 us: passed_along(): return lax.ppermute(shard, axis, pairs)]
    slice x13 -> x0, local copies, waits for them, and re-layouts: 4.56 us -> none  [the longest x4 1.64 us: windowed_attention(): band_keys = jnp.concatenate([key_matrix[:-1], key_matrix[1:]], axis=1)]
    convert_element_type x4 -> x0, other arithmetic: 4.55 us -> none  [the longest x2 2.65 us: rounded(): return lax.optimization_barrier(value.astype(jnp.bfloat16))]
  transfers between devices with their start and end apart: 8 -> 0, of which waited for: 5 -> 0; matrix products, arithmetic and copies ran while one was open for 12% -> 0% of each run, Pallas kernels for 0% -> 0%
where the time goes in v1:
time: 174 us
  Pallas kernels  170 us (98%)
  local copies, waits for them, and re-layouts  3.79 us (2%)
    pallas_call x1, Pallas kernels, kernel_body(): pl.pallas_call(functools.partial(layer_kernel, n_z), out_shape=jax.ShapeD...  170 us

profile of v1, /device:TPU:0, one launch (start us, length us, event | category | flops | bytes accessed | tf_op | source)
XLA Modules:
  0.0 173.7 jit_solution(15727799105875059618)
XLA Ops:
  0.0 1.3 reshape.6.docs_hbm
  1.3 169.9 %shard_map.100 = bf16[320,2048]{1,0:T(8,128)(2,1)} custom-call(bf16[640,512]{1,0:T(8,128)(2,1)} %q_hbm.1, bf16[640,128]{1,0:T(8,128)(2,1)} %k_hbm.1, bf16[640,128]{1,0:T(8,128)(2,1)} %v_hbm.1, s32[5,1,128]{2,1,0:T(1,128)} %reshape.6.docs_hbm, f32[8]{0:T(128)} %sinks.1, bf16[1024,2048]{1,0:T(8,128)(2,1)} %outw_hbm.1, bf16[320,2048]{1,0:T(8,128)(2,1)} %res_hbm.1, ...), custom_call_target="tpu_custom_call" | custom-call | tf_op jit(solution)/shard_map/pallas_call | solution.py:563
  171.2 2.5 %copy.12 = bf16[320,2048]{1,0:T(8,128)(2,1)} copy(bf16[320,2048]{1,0:T(8,128)(2,1)} %shard_map.100) | data formatting | bytes 2621440

commit v2 on v1

--- a/solution.py
+++ b/solution.py
@@ -144,6 +144,7 @@
     return (
         n_tp == 2
         and n_sp % (n_tp * CORES) == 0
+        and n_sp // (n_tp * CORES) >= 3
         and block % LANES == 0
         and kv_width == LANES
         and width % (2 * LANES) == 0
@@ -155,11 +156,11 @@
 
 def layer_kernel(
     n_z,
-    q_hbm, k_hbm, v_hbm, docs_hbm, sinks, outw_hbm, res_hbm, gain_ref, up_hbm, down_hbm,
-    out_hbm,
-    up_all, down_all, rows_all, hid_all, outw, res, mixed, q_ref, k_ref, v_ref, docs,
-    k_wide, v_wide, att, oth, psend, precv, own_sum, out_ref,
-    load_sem, halo_send, halo_recv, xs_sem, z_send, z_recv, d_send, d_recv, y_sem,
+    q_hbm, k_hbm, v_hbm, docs_flat, sinks, outw_hbm, res_hbm, gain_ref, up_hbm, down_hbm,
+    out_ref,
+    up_all, down_all, rows_all, hid_all, outw, res, mixed, q_ref, k_ref, v_ref, docs, docs_prev,
+    k_wide, v_wide, att, oth, psend, precv, own_sum,
+    load_sem, halo_send, halo_recv, xs_sem, xr_sem, z_send, z_recv, d_send, d_recv, y_sem,
     g_send, g_recv, p_send, p_recv, own_sem,
 ):
     sp, y = lax.axis_index("sp"), lax.axis_index("tp")
@@ -197,18 +198,24 @@
             return up_hbm.at[:, pl.ds(start, quarter)]
         return down_hbm.at[pl.ds(start, quarter), :]
 
-    def x_exchange(phase):
+    def part_of(ref, h):
+        size = ref.shape[0] // 2
+        return ref.at[pl.ds(h * size, size), :]
+
+    def x_exchange(phase, h):
         return remote(
-            own_piece(phase, 1 - x), block(phase, z, x, c), xs_sem.at[phase], z_recv.at[phase, z, 1], x_peer
+            part_of(own_piece(phase, 1 - x), h), part_of(block(phase, z, x, c), h),
+            xs_sem.at[phase, h], xr_sem.at[phase, h], x_peer,
         )
 
     def own_load(phase):
         return pltpu.make_async_copy(own_piece(phase, x), block(phase, z, x, c), own_sem.at[phase])
 
     low = jnp.minimum(z, n_z - 1 - z)
+    inward = jnp.where(2 * z < n_z, 1, -1)
 
     def plane(k):
-        near = jnp.where(lax.rem(k, 2) == 1, z - (k + 1) // 2, z + (k + 1) // 2)
+        near = z + jnp.where(lax.rem(k, 2) == 1, inward, -inward) * ((k + 1) // 2)
         far = jnp.where(z < n_z - 1 - z, k, n_z - 1 - k)
         return jnp.where(k <= 2 * low, near, far)
 
@@ -246,6 +253,25 @@
             to_down(phase, zb, b, xb).start()
 
         to_core(phase, zb, b, xb).start()
+
+    def arrive_x(phase, h):
+        x_exchange(phase, h).wait_recv()
+        ref = part_of(block(phase, z, 1 - x, c), h)
+
+        @pl.when(z < n_z - 1)
+        def _():
+            remote(
+                ref, ref, z_send.at[0, phase, z, 1], z_recv.at[phase, z, 1], at(z + 1, x, y, c)
+            ).start()
+
+        @pl.when(z > 0)
+        def _():
+            remote(
+                ref, ref, z_send.at[1, phase, z, 1], z_recv.at[phase, z, 1], at(z - 1, x, y, c)
+            ).start()
+
+        if h == 1:
+            to_core(phase, z, 1, 1 - x).start()
 
     def arrive(phase, t):
         zb, b, xb = place(t)
@@ -259,45 +285,71 @@
         src, dst = (
             (k_hbm.at[pl.ds(last, WINDOW_REACH), :], k_ref.at[pl.ds(0, WINDOW_REACH), :]),
             (v_hbm.at[pl.ds(last, WINDOW_REACH), :], v_ref.at[pl.ds(0, WINDOW_REACH), :]),
-            (docs_hbm.at[last // LANES], docs.at[0]),
+            (docs_flat, docs_prev),
         )[i]
         return remote(src, dst, halo_send.at[i], halo_recv.at[i], nxt)
+
+    own_load(0).start()
+    barrier = pltpu.get_barrier_semaphore()
+    partners = (
+        (True, x_peer), (True, y_peer), (True, at(z, 1 - x, 1 - y, c)), (True, c_peer),
+        (z < n_z - 1, at(z + 1, x, y, c)), (z > 0, at(z - 1, x, y, c)),
+        (sp < n_sp - 1, nxt), (sp > 0, (sp - 1, y)),
+    )
+    for here, dev in partners:
+        @pl.when(here)
+        def _():
+            pl.semaphore_signal(barrier, inc=1, device_id=dev, device_id_type=MESH)
+
+    pl.semaphore_wait(barrier, sum(jnp.int32(here) for here, _ in partners))
 
     @pl.when(sp < n_sp - 1)
     def _():
         for i in range(3):
             halo(i).start()
 
-    own_load(0).start()
     loads = [
         pltpu.make_async_copy(q_hbm, q_ref, load_sem.at[0]),
         pltpu.make_async_copy(k_hbm, k_ref.at[pl.ds(WINDOW_REACH, tokens), :], load_sem.at[1]),
         pltpu.make_async_copy(v_hbm, v_ref.at[pl.ds(WINDOW_REACH, tokens), :], load_sem.at[2]),
-        pltpu.make_async_copy(docs_hbm, docs.at[pl.ds(1, tokens // LANES)], load_sem.at[3]),
-        pltpu.make_async_copy(outw_hbm, outw, load_sem.at[4]),
-        pltpu.make_async_copy(res_hbm, res, load_sem.at[5]),
+        pltpu.make_async_copy(outw_hbm, outw, load_sem.at[3]),
+        pltpu.make_async_copy(res_hbm, res, load_sem.at[4]),
     ]
-    x_exchange(0).start()
     own_load(0).wait()
-    pass_on(0, 0)
+
+    def begin():
+        x_exchange(0, 0).start()
+        pass_on(0, 0)
+        x_exchange(0, 1).start()
+
+    @pl.when(c == 1)
+    def _():
+        begin()
+
     for load in loads:
         load.start()
     own_load(1).start()
-    x_exchange(1).start()
 
     @pl.when(sp == 0)
     def _():
         k_ref[pl.ds(0, WINDOW_REACH), :] = jnp.zeros((WINDOW_REACH, LANES), jnp.bfloat16)
         v_ref[pl.ds(0, WINDOW_REACH), :] = jnp.zeros((WINDOW_REACH, LANES), jnp.bfloat16)
-        docs[0] = jnp.full(docs.shape[1:], -1, jnp.int32)
-
-    for load in loads[:4]:
+        docs_prev[...] = jnp.full(docs_prev.shape, -1, jnp.int32)
+
+    for load in loads[:3]:
         load.wait()
 
     @pl.when(sp > 0)
     def _():
         for i in range(3):
             halo(i).wait_recv()
+
+    docs[0, 0] = docs_prev[last:]
+    for i in range(tokens // LANES):
+        docs[i + 1, 0] = docs_flat[i * LANES : (i + 1) * LANES]
+    @pl.when(c == 0)
+    def _():
+        begin()
 
     heads = width // HEAD_SIZE
     kv_heads = LANES // HEAD_SIZE
@@ -348,18 +400,26 @@
             att[pl.ds(start, WINDOW_REACH), j * LANES : (j + 1) * LANES] = total_out.astype(
                 jnp.bfloat16
             )
+
+        @pl.when(n == steps // 2 + 1)
+        def _():
+            arrive_x(0, 0)
+
         return carry
 
-    lax.fori_loop(0, tokens // WINDOW_REACH, attend, 0)
+    steps = tokens // WINDOW_REACH
+    lax.fori_loop(0, steps, attend, 0)
 
     mine_at = pl.multiple_of(y * rows, rows)
     theirs_at = pl.multiple_of((1 - y) * rows, rows)
     swap = remote(att.at[pl.ds(theirs_at, rows), :], oth, y_sem.at[0], y_sem.at[1], y_peer)
     swap.start()
-    arrive(0, 1)
+    for h in range(2):
+        x_exchange(1, h).start()
+    arrive_x(0, 1)
     arrive(0, 2)
+    loads[3].wait()
     loads[4].wait()
-    loads[5].wait()
     swap.wait_recv()
 
     me_p = x * n_y + y
@@ -427,7 +487,8 @@
 
     own_load(1).wait()
     pass_on(1, 0)
-    arrive(1, 1)
+    for h in range(2):
+        arrive_x(1, h)
 
     give(x_p, 1, 0).wait_recv()
     give(y_p, 0, 1).wait_recv()
@@ -454,65 +515,87 @@
 
     lax.fori_loop(0, 2 * (quarter // chunk), up_step, 0)
 
-    def partial_copy(j, s):
-        px, py = jnp.where(s >= 2, 1 - x, x), jnp.where(lax.rem(s, 2) == 1, 1 - y, y)
+    def lanes(ref, h):
+        return ref if h is None else ref.at[:, pl.ds(h * blk, blk)]
+
+    def way(s):
+        return jnp.where(s >= 2, 1 - x, x), jnp.where(lax.rem(s, 2) == 1, 1 - y, y)
+
+    def partial_copy(j, s, h=None):
+        px, py = way(s)
         return remote(
-            psend.at[j, s - 1], precv.at[j, s - 1], p_send.at[j, s - 1], p_recv.at[j, s - 1], at(z, px, py, c)
+            lanes(psend.at[j, s - 1], h), lanes(precv.at[j, s - 1], h),
+            p_send.at[j, h or 0, s - 1], p_recv.at[j, h or 0, s - 1], at(z, px, py, c),
         )
 
-    def combine(t):
+    def pair_of(t):
         zb, b, xb = place(t)
-        j = zb * n_x + xb
-        total = own_sum[j]
+        return zb * n_x + xb
+
+    def combine(t, h=None):
+        j = pair_of(t)
+        total = lanes(own_sum.at[j], h)[...]
         for s in (1, 2, 3):
-            partial_copy(j, s).wait_recv()
-            total = total + precv[j, s - 1].astype(jnp.float32)
-        cols = pl.ds(pl.multiple_of(j * wide, wide), wide)
+            partial_copy(j, s, h).wait_recv()
+            total = total + lanes(precv.at[j, s - 1], h)[...].astype(jnp.float32)
+        size = wide if h is None else blk
+        cols = pl.ds(pl.multiple_of(j * wide + (h or 0) * blk, blk), size)
         out_ref[:, cols] = (
             mixed[:, cols].astype(jnp.float32) + total.astype(jnp.bfloat16).astype(jnp.float32)
         ).astype(jnp.bfloat16)
 
-    def down_step(t, carry):
-        @pl.when(t >= 2)
-        def _():
-            arrive(1, t)
-
-        zb, b, xb = place(t)
-        to_core(1, zb, b, xb).wait_recv()
-        j = zb * n_x + xb
-
+    def pieces(j, h=None):
         def piece(i, carry):
             s = 3 - i
-            px, py = jnp.where(s >= 2, 1 - x, x), jnp.where(lax.rem(s, 2) == 1, 1 - y, y)
+            px, py = way(s)
             first = pl.multiple_of((px * n_y + py) * rows, rows)
             part = jnp.dot(
-                hid_all[pl.ds(first, rows), :], down_all[j], preferred_element_type=jnp.float32
+                hid_all[pl.ds(first, rows), :], lanes(down_all.at[j], h)[...],
+                preferred_element_type=jnp.float32,
             )
 
             @pl.when(s > 0)
             def _():
-                psend[j, s - 1] = part.astype(jnp.bfloat16)
-                partial_copy(j, s).start()
+                lanes(psend.at[j, s - 1], h)[...] = part.astype(jnp.bfloat16)
+                partial_copy(j, s, h).start()
 
             @pl.when(s == 0)
             def _():
-                own_sum[j] = part
+                lanes(own_sum.at[j], h)[...] = part
 
             return carry
 
         lax.fori_loop(0, n_x * n_y, piece, 0)
 
-        @pl.when(t >= 2)
-        def _():
-            combine(t - 2)
+    lag = 4
+    n_whole = n_items - 2
+
+    def blocks_sent(phase, t):
+        zb, b, xb = place(t)
+
+        @pl.when(goes_up(zb))
+        def _():
+            to_up(phase, zb, b, xb).wait_send()
+
+        @pl.when(goes_down(zb))
+        def _():
+            to_down(phase, zb, b, xb).wait_send()
+
+        to_core(phase, zb, b, xb).wait_send()
+
+    def partials_sent(t, carry):
+        j = pair_of(t)
+        for s in (1, 2, 3):
+            @pl.when(t < n_whole)
+            def _():
+                partial_copy(j, s).wait_send()
+
+            @pl.when(t >= n_whole)
+            def _():
+                for h in range(2):
+                    partial_copy(j, s, h).wait_send()
 
         return carry
-
-    lax.fori_loop(0, n_items, down_step, 0)
-    for t in (n_items - 2, n_items - 1):
-        combine(jnp.int32(t))
-    store = pltpu.make_async_copy(out_ref, out_hbm, load_sem.at[0])
-    store.start()
 
     @pl.when(sp < n_sp - 1)
     def _():
@@ -521,31 +604,67 @@
 
     swap.wait_send()
     for phase in range(2):
-        x_exchange(phase).wait_send()
+        for h in range(2):
+            x_exchange(phase, h).wait_send()
+
+    def down_step(t, carry):
+        @pl.when(t >= 2)
+        def _():
+            arrive(1, t)
+
+        zb, b, xb = place(t)
+        to_core(1, zb, b, xb).wait_recv()
+        pieces(pair_of(t))
+
+        @pl.when(t >= lag)
+        def _():
+            combine(t - lag)
+            partials_sent(t - lag, 0)
+
+        blocks_sent(0, t)
+        return carry
+
+    lax.fori_loop(0, n_whole, down_step, 0)
+
+    def last_step(t, carry):
+        for h in (1, 0):
+            @pl.when(c == h)
+            def _():
+                arrive(1, t)
+
+            @pl.when(c != h)
+            def _():
+                zb, b, xb = place(t)
+                to_core(1, zb, b, xb).wait_recv()
+
+            pieces(pair_of(t), h)
+            done = n_whole - lag + 2 * (t - n_whole) + 1 - h
+
+            @pl.when(done < n_whole - 1)
+            def _():
+                combine(done)
+                partials_sent(done, 0)
+
+        blocks_sent(0, t)
+        return carry
+
+    lax.fori_loop(n_whole, n_items, last_step, 0)
     for h in range(2):
         give(me_p, h, 0).wait_send()
         give(me_p, h, 1).wait_send()
     give(x_p, 0, 1).wait_send()
     give(y_p, 1, 0).wait_send()
 
-    def sent(t, carry):
-        zb, b, xb = place(t)
-        for phase in range(2):
-            @pl.when(goes_up(zb))
-            def _():
-                to_up(phase, zb, b, xb).wait_send()
-
-            @pl.when(goes_down(zb))
-            def _():
-                to_down(phase, zb, b, xb).wait_send()
-
-            to_core(phase, zb, b, xb).wait_send()
-        for s in (1, 2, 3):
-            partial_copy(zb * n_x + xb, s).wait_send()
+    def down_sent(t, carry):
+        blocks_sent(1, t)
         return carry
 
-    lax.fori_loop(0, n_items, sent, 0)
-    store.wait()
+    lax.fori_loop(0, n_items, down_sent, 0)
+    for t in range(n_whole - 1, n_items):
+        for h in (None,) if t < n_whole else (1, 0):
+            combine(jnp.int32(t), h)
+
+    lax.fori_loop(n_whole - 1, n_items, partials_sent, 0)
 
 
 def kernel_body(
@@ -562,10 +681,10 @@
     dma = pltpu.SemaphoreType.DMA
     return pl.pallas_call(
         functools.partial(layer_kernel, n_z),
-        out_shape=jax.ShapeDtypeStruct((rows, model), bf16),
-        in_specs=[hbm, hbm, hbm, hbm, pl.BlockSpec(memory_space=pltpu.SMEM), hbm, hbm,
+        out_shape=pltpu.VMEM((rows, model), bf16),
+        in_specs=[hbm, hbm, hbm, pl.BlockSpec(memory_space=pltpu.VMEM), pl.BlockSpec(memory_space=pltpu.SMEM), hbm, hbm,
                   pl.BlockSpec(memory_space=pltpu.VMEM), hbm, hbm],
-        out_specs=hbm,
+        out_specs=pl.BlockSpec(memory_space=pltpu.VMEM),
         scratch_shapes=[
             pltpu.VMEM((model, quarter), bf16),
             pltpu.VMEM((pairs, quarter, 2 * blk), bf16),
@@ -578,6 +697,7 @@
             pltpu.VMEM((tokens + WINDOW_REACH, LANES), bf16),
             pltpu.VMEM((tokens + WINDOW_REACH, LANES), bf16),
             pltpu.VMEM((tokens // LANES + 1, 1, LANES), jnp.int32),
+            pltpu.VMEM((tokens,), jnp.int32),
             pltpu.VMEM((4, tokens + WINDOW_REACH, LANES), bf16),
             pltpu.VMEM((4, tokens + WINDOW_REACH, LANES), bf16),
             pltpu.VMEM((tokens, width), bf16),
@@ -585,14 +705,13 @@
             pltpu.VMEM((pairs, 3, rows, 2 * blk), bf16),
             pltpu.VMEM((pairs, 3, rows, 2 * blk), bf16),
             pltpu.VMEM((pairs, rows, 2 * blk), f32),
-            pltpu.VMEM((rows, model), bf16),
-            dma((6,)), dma((3,)), dma((3,)), dma((2,)), dma((2, 2, n_z, 2)), dma((2, n_z, 2)),
+            dma((6,)), dma((3,)), dma((3,)), dma((2, 2)), dma((2, 2)), dma((2, 2, n_z, 2)), dma((2, n_z, 2)),
             dma((2, n_z, 2)), dma((2, n_z, 2)), dma((2,)), dma((2, 8)), dma((8,)),
-            dma((pairs, 3)), dma((pairs, 3)), dma((2,)),
+            dma((pairs, 2, 3)), dma((pairs, 2, 3)), dma((2,)),
         ],
-        compiler_params=pltpu.CompilerParams(has_side_effects=True, vmem_limit_bytes=67043328),
+        compiler_params=pltpu.CompilerParams(collective_id=0, has_side_effects=True, vmem_limit_bytes=60 << 20),
     )(
-        queries, keys, values, documents.reshape(tokens // LANES, 1, LANES), sinks, out_weight,
+        queries, keys, values, documents, sinks, out_weight,
         residual, norm_gain.reshape(1, model), up_weight, down_weight,
     )
 

time: 174 us -> 153 us (0.88)
  Pallas kernels: 170 us -> 152 us
  local copies, waits for them, and re-layouts: 3.79 us -> 1.06 us
    pallas_call x1, Pallas kernels: 170 us -> 152 us  [kernel_body(): pl.pallas_call(functools.partial(layer_kernel, n_z), out_shape=pltpu.VMEM...]
where the time goes in v2:
time: 153 us
  Pallas kernels  152 us (99%)
    pallas_call x1, Pallas kernels, kernel_body(): pl.pallas_call(functools.partial(layer_kernel, n_z), out_shape=pltpu.VMEM...  152 us

profile of v2, /device:TPU:0, one launch (start us, length us, event | category | flops | bytes accessed | tf_op | source)
XLA Modules:
  0.0 153.1 jit_solution(3738238547060495307)
XLA Ops:
  0.0 152.1 %shard_map.100 = bf16[320,2048]{1,0:T(8,128)(2,1)S(1)} custom-call(bf16[640,512]{1,0:T(8,128)(2,1)} %q_hbm.1, bf16[640,128]{1,0:T(8,128)(2,1)} %k_hbm.1, bf16[640,128]{1,0:T(8,128)(2,1)} %v_hbm.1, s32[640]{0:T(1024)} %docs_flat.1, f32[8]{0:T(128)} %sinks.1, bf16[1024,2048]{1,0:T(8,128)(2,1)} %outw_hbm.1, bf16[320,2048]{1,0:T(8,128)(2,1)} %res_hbm.1, ...), custom_call_target="tpu_custom_call" | custom-call | tf_op jit(solution)/shard_map/pallas_call | solution.py:682
  152.1 1.1 copy.12

commit v3 on v2

--- a/solution.py
+++ b/solution.py
@@ -156,9 +156,9 @@
 
 def layer_kernel(
     n_z,
-    q_hbm, k_hbm, v_hbm, docs_flat, sinks, outw_hbm, res_hbm, gain_ref, up_hbm, down_hbm,
+    q_hbm, k_hbm, v_hbm, docs_hbm, sinks_hbm, outw_hbm, res_hbm, gain_hbm, up_hbm, down_hbm,
     out_ref,
-    up_all, down_all, rows_all, hid_all, outw, res, mixed, q_ref, k_ref, v_ref, docs, docs_prev,
+    up_all, down_all, rows_all, hid_all, outw, res, mixed, q_ref, k_ref, v_ref, docs, docs_prev, docs_flat, sinks, gain_ref,
     k_wide, v_wide, att, oth, psend, precv, own_sum,
     load_sem, halo_send, halo_recv, xs_sem, xr_sem, z_send, z_recv, d_send, d_recv, y_sem,
     g_send, g_recv, p_send, p_recv, own_sem,
@@ -205,7 +205,7 @@
     def x_exchange(phase, h):
         return remote(
             part_of(own_piece(phase, 1 - x), h), part_of(block(phase, z, x, c), h),
-            xs_sem.at[phase, h], xr_sem.at[phase, h], x_peer,
+            xs_sem.at[phase], xr_sem.at[phase, h], x_peer,
         )
 
     def own_load(phase):
@@ -225,15 +225,20 @@
 
     def to_up(phase, zb, b, xb):
         ref = block(phase, zb, xb, c)
-        return remote(ref, ref, z_send.at[0, phase, zb, b], z_recv.at[phase, zb, b], at(z + 1, x, y, c))
+        return remote(ref, ref, z_send.at[phase], z_recv.at[phase, zb, b], at(z + 1, x, y, c))
 
     def to_down(phase, zb, b, xb):
         ref = block(phase, zb, xb, c)
-        return remote(ref, ref, z_send.at[1, phase, zb, b], z_recv.at[phase, zb, b], at(z - 1, x, y, c))
+        return remote(ref, ref, z_send.at[phase], z_recv.at[phase, zb, b], at(z - 1, x, y, c))
 
     def to_core(phase, zb, b, xb):
         ref = block(phase, zb, xb, c)
-        return remote(ref, ref, d_send.at[phase, zb, b], d_recv.at[phase, zb, b], c_peer)
+        slot = 0 if phase == 0 else 1 + zb * n_x + b
+        return remote(ref, ref, d_send.at[phase], d_recv.at[slot], c_peer)
+
+    def to_core_all(phase):
+        ref = up_all.at[pl.ds(0, model // 2), :] if phase == 0 else down_all.at[pl.ds(0, n_z)]
+        return remote(ref, ref, d_send.at[phase], d_recv.at[0], c_peer)
 
     def goes_up(zb):
         return jnp.logical_and(zb <= z, z < n_z - 1)
@@ -261,13 +266,13 @@
         @pl.when(z < n_z - 1)
         def _():
             remote(
-                ref, ref, z_send.at[0, phase, z, 1], z_recv.at[phase, z, 1], at(z + 1, x, y, c)
+                ref, ref, z_send.at[phase], z_recv.at[phase, z, 1], at(z + 1, x, y, c)
             ).start()
 
         @pl.when(z > 0)
         def _():
             remote(
-                ref, ref, z_send.at[1, phase, z, 1], z_recv.at[phase, z, 1], at(z - 1, x, y, c)
+                ref, ref, z_send.at[phase], z_recv.at[phase, z, 1], at(z - 1, x, y, c)
             ).start()
 
         if h == 1:
@@ -285,7 +290,7 @@
         src, dst = (
             (k_hbm.at[pl.ds(last, WINDOW_REACH), :], k_ref.at[pl.ds(0, WINDOW_REACH), :]),
             (v_hbm.at[pl.ds(last, WINDOW_REACH), :], v_ref.at[pl.ds(0, WINDOW_REACH), :]),
-            (docs_flat, docs_prev),
+            (docs_hbm, docs_prev),
         )[i]
         return remote(src, dst, halo_send.at[i], halo_recv.at[i], nxt)
 
@@ -314,6 +319,9 @@
         pltpu.make_async_copy(v_hbm, v_ref.at[pl.ds(WINDOW_REACH, tokens), :], load_sem.at[2]),
         pltpu.make_async_copy(outw_hbm, outw, load_sem.at[3]),
         pltpu.make_async_copy(res_hbm, res, load_sem.at[4]),
+        pltpu.make_async_copy(gain_hbm, gain_ref, load_sem.at[5]),
+        pltpu.make_async_copy(docs_hbm, docs_flat, load_sem.at[6]),
+        pltpu.make_async_copy(sinks_hbm, sinks, load_sem.at[7]),
     ]
     own_load(0).wait()
 
@@ -336,7 +344,7 @@
         v_ref[pl.ds(0, WINDOW_REACH), :] = jnp.zeros((WINDOW_REACH, LANES), jnp.bfloat16)
         docs_prev[...] = jnp.full(docs_prev.shape, -1, jnp.int32)
 
-    for load in loads[:3]:
+    for load in loads[:3] + loads[6:]:
         load.wait()
 
     @pl.when(sp > 0)
@@ -418,8 +426,8 @@
         x_exchange(1, h).start()
     arrive_x(0, 1)
     arrive(0, 2)
-    loads[3].wait()
-    loads[4].wait()
+    for load in loads[3:6]:
+        load.wait()
     swap.wait_recv()
 
     me_p = x * n_y + y
@@ -430,9 +438,8 @@
         return rows_all.at[pl.ds(pl.multiple_of(p * rows + h * half, half), half), :]
 
     def give(p, h, way):
-        slot = p * 2 + h
         ref = row_part(p, h)
-        return remote(ref, ref, g_send.at[way, slot], g_recv.at[slot], x_peer if way == 0 else y_peer)
+        return remote(ref, ref, g_send.at[0], g_recv.at[p * 2 + h], x_peer if way == 0 else y_peer)
 
     for h in range(2):
         own_rows = pl.ds(pl.multiple_of(mine_at + h * half, half), half)
@@ -495,14 +502,7 @@
     give(d_p, 0, 1).wait_recv()
     give(d_p, 1, 0).wait_recv()
 
-    def core_wait(phase):
-        def wait_one(t, carry):
-            zb, b, xb = place(t)
-            to_core(phase, zb, b, xb).wait_recv()
-            return carry
-        return wait_one
-
-    lax.fori_loop(0, n_items, core_wait(0), 0)
+    to_core_all(0).wait_recv()
     tall = 2 * rows
 
     def up_step(i, carry):
@@ -516,7 +516,13 @@
     lax.fori_loop(0, 2 * (quarter // chunk), up_step, 0)
 
     def lanes(ref, h):
-        return ref if h is None else ref.at[:, pl.ds(h * blk, blk)]
+        if h is None:
+            return ref
+        cut = pl.ds(h * blk, blk)
+        return ref.at[:, cut] if len(ref.shape) == 2 else ref.at[:, :, cut]
+
+    def partial_slot(j, h):
+        return 2 * n_z + lax.rem(j, n_x) if h == 0 else j
 
     def way(s):
         return jnp.where(s >= 2, 1 - x, x), jnp.where(lax.rem(s, 2) == 1, 1 - y, y)
@@ -525,7 +531,13 @@
         px, py = way(s)
         return remote(
             lanes(psend.at[j, s - 1], h), lanes(precv.at[j, s - 1], h),
-            p_send.at[j, h or 0, s - 1], p_recv.at[j, h or 0, s - 1], at(z, px, py, c),
+            p_send.at[0], p_recv.at[partial_slot(j, h)], at(z, px, py, c),
+        )
+
+    def partials(j, h=None):
+        return remote(
+            lanes(psend.at[j], h), lanes(precv.at[j], h),
+            p_send.at[0], p_recv.at[partial_slot(j, h)], x_peer,
         )
 
     def pair_of(t):
@@ -535,8 +547,8 @@
     def combine(t, h=None):
         j = pair_of(t)
         total = lanes(own_sum.at[j], h)[...]
+        partials(j, h).wait_recv()
         for s in (1, 2, 3):
-            partial_copy(j, s, h).wait_recv()
             total = total + lanes(precv.at[j, s - 1], h)[...].astype(jnp.float32)
         size = wide if h is None else blk
         cols = pl.ds(pl.multiple_of(j * wide + (h or 0) * blk, blk), size)
@@ -570,32 +582,17 @@
     lag = 4
     n_whole = n_items - 2
 
-    def blocks_sent(phase, t):
-        zb, b, xb = place(t)
-
-        @pl.when(goes_up(zb))
-        def _():
-            to_up(phase, zb, b, xb).wait_send()
-
-        @pl.when(goes_down(zb))
-        def _():
-            to_down(phase, zb, b, xb).wait_send()
-
-        to_core(phase, zb, b, xb).wait_send()
-
-    def partials_sent(t, carry):
-        j = pair_of(t)
-        for s in (1, 2, 3):
-            @pl.when(t < n_whole)
+    def line_sent(phase):
+        for here in range(n_z):
+            blocks = 2 * (here + 1) * (here < n_z - 1) + 2 * (n_z - here) * (here > 0)
+
+            @pl.when(z == here)
             def _():
-                partial_copy(j, s).wait_send()
-
-            @pl.when(t >= n_whole)
-            def _():
-                for h in range(2):
-                    partial_copy(j, s, h).wait_send()
-
-        return carry
+                if phase == 0:
+                    ref = up_all.at[pl.ds(0, blocks * blk), :]
+                else:
+                    ref = down_all.at[pl.ds(0, blocks // 2)]
+                remote(ref, ref, z_send.at[phase], z_recv.at[phase, 0, 0], x_peer).wait_send()
 
     @pl.when(sp < n_sp - 1)
     def _():
@@ -604,8 +601,8 @@
 
     swap.wait_send()
     for phase in range(2):
-        for h in range(2):
-            x_exchange(phase, h).wait_send()
+        whole = block(phase, z, x, c)
+        remote(whole, whole, xs_sem.at[phase], xr_sem.at[phase, 0], x_peer).wait_send()
 
     def down_step(t, carry):
         @pl.when(t >= 2)
@@ -619,9 +616,7 @@
         @pl.when(t >= lag)
         def _():
             combine(t - lag)
-            partials_sent(t - lag, 0)
-
-        blocks_sent(0, t)
+
         return carry
 
     lax.fori_loop(0, n_whole, down_step, 0)
@@ -643,28 +638,22 @@
             @pl.when(done < n_whole - 1)
             def _():
                 combine(done)
-                partials_sent(done, 0)
-
-        blocks_sent(0, t)
+
         return carry
 
+    line_sent(0)
     lax.fori_loop(n_whole, n_items, last_step, 0)
-    for h in range(2):
-        give(me_p, h, 0).wait_send()
-        give(me_p, h, 1).wait_send()
-    give(x_p, 0, 1).wait_send()
-    give(y_p, 1, 0).wait_send()
-
-    def down_sent(t, carry):
-        blocks_sent(1, t)
-        return carry
-
-    lax.fori_loop(0, n_items, down_sent, 0)
+    given = rows_all.at[pl.ds(0, 3 * rows), :]
+    remote(given, given, g_send.at[0], g_recv.at[0], x_peer).wait_send()
+    line_sent(1)
+    for phase in range(2):
+        to_core_all(phase).wait_send()
+
     for t in range(n_whole - 1, n_items):
         for h in (None,) if t < n_whole else (1, 0):
             combine(jnp.int32(t), h)
 
-    lax.fori_loop(n_whole - 1, n_items, partials_sent, 0)
+    remote(psend, precv, p_send.at[0], p_recv.at[0], x_peer).wait_send()
 
 
 def kernel_body(
@@ -682,8 +671,7 @@
     return pl.pallas_call(
         functools.partial(layer_kernel, n_z),
         out_shape=pltpu.VMEM((rows, model), bf16),
-        in_specs=[hbm, hbm, hbm, pl.BlockSpec(memory_space=pltpu.VMEM), pl.BlockSpec(memory_space=pltpu.SMEM), hbm, hbm,
-                  pl.BlockSpec(memory_space=pltpu.VMEM), hbm, hbm],
+        in_specs=[hbm] * 10,
         out_specs=pl.BlockSpec(memory_space=pltpu.VMEM),
         scratch_shapes=[
             pltpu.VMEM((model, quarter), bf16),
@@ -698,6 +686,9 @@
             pltpu.VMEM((tokens + WINDOW_REACH, LANES), bf16),
             pltpu.VMEM((tokens // LANES + 1, 1, LANES), jnp.int32),
             pltpu.VMEM((tokens,), jnp.int32),
+            pltpu.VMEM((tokens,), jnp.int32),
+            pltpu.SMEM(sinks.shape, f32),
+            pltpu.VMEM((1, model), f32),
             pltpu.VMEM((4, tokens + WINDOW_REACH, LANES), bf16),
             pltpu.VMEM((4, tokens + WINDOW_REACH, LANES), bf16),
             pltpu.VMEM((tokens, width), bf16),
@@ -705,9 +696,9 @@
             pltpu.VMEM((pairs, 3, rows, 2 * blk), bf16),
             pltpu.VMEM((pairs, 3, rows, 2 * blk), bf16),
             pltpu.VMEM((pairs, rows, 2 * blk), f32),
-            dma((6,)), dma((3,)), dma((3,)), dma((2, 2)), dma((2, 2)), dma((2, 2, n_z, 2)), dma((2, n_z, 2)),
-            dma((2, n_z, 2)), dma((2, n_z, 2)), dma((2,)), dma((2, 8)), dma((8,)),
-            dma((pairs, 2, 3)), dma((pairs, 2, 3)), dma((2,)),
+            dma((8,)), dma((3,)), dma((3,)), dma((2,)), dma((2, 2)), dma((2,)), dma((2, n_z, 2)),
+            dma((2,)), dma((1 + 2 * n_z,)), dma((2,)), dma((1,)), dma((8,)),
+            dma((1,)), dma((pairs + 2,)), dma((2,)),
         ],
         compiler_params=pltpu.CompilerParams(collective_id=0, has_side_effects=True, vmem_limit_bytes=60 << 20),
     )(

time: 153 us -> 152 us (level)
  Pallas kernels: 152 us -> 150 us
    pallas_call x1, Pallas kernels: 152 us -> 150 us  [kernel_body(): pl.pallas_call(functools.partial(layer_kernel, n_z), out_shape=pltpu.VMEM...]
where the time goes in v3:
time: 152 us; the launch traced here: 151 us
  Pallas kernels  150 us (99%)
    pallas_call x1, Pallas kernels, kernel_body(): pl.pallas_call(functools.partial(layer_kernel, n_z), out_shape=pltpu.VMEM...  150 us

profile of v3, /device:TPU:0, one launch (start us, length us, event | category | flops | bytes accessed | tf_op | source)
XLA Modules:
  0.0 151.4 jit_solution(3420441506143728599)
XLA Ops:
  0.0 150.3 %shard_map.100 = bf16[320,2048]{1,0:T(8,128)(2,1)S(1)} custom-call(bf16[640,512]{1,0:T(8,128)(2,1)} %q_hbm.1, bf16[640,128]{1,0:T(8,128)(2,1)} %k_hbm.1, bf16[640,128]{1,0:T(8,128)(2,1)} %v_hbm.1, s32[640]{0:T(1024)} %docs_hbm.1, f32[8]{0:T(128)} %sinks_hbm.1, bf16[1024,2048]{1,0:T(8,128)(2,1)} %outw_hbm.1, bf16[320,2048]{1,0:T(8,128)(2,1)} %res_hbm.1, ...), custom_call_target="tpu_custom_call" | custom-call | tf_op jit(solution)/shard_map/pallas_call | solution.py:671
  150.3 1.1 copy.12

commit v4 on v3

--- a/solution.py
+++ b/solution.py
@@ -558,7 +558,7 @@
 
     def pieces(j, h=None):
         def piece(i, carry):
-            s = 3 - i
+            s = jnp.where(i == 0, 1, jnp.where(i == 1, 3, jnp.where(i == 2, 2, 0)))
             px, py = way(s)
             first = pl.multiple_of((px * n_y + py) * rows, rows)
             part = jnp.dot(

time: 152 us -> 151 us (level)
    pallas_call x1, Pallas kernels: 150 us -> 149 us  [kernel_body(): pl.pallas_call(functools.partial(layer_kernel, n_z), out_shape=pltpu.VMEM...]
where the time goes in v4:
time: 151 us; the launch traced here: 150 us
  Pallas kernels  149 us (99%)
    pallas_call x1, Pallas kernels, kernel_body(): pl.pallas_call(functools.partial(layer_kernel, n_z), out_shape=pltpu.VMEM...  149 us

profile of v4, /device:TPU:0, one launch (start us, length us, event | category | flops | bytes accessed | tf_op | source)
XLA Modules:
  0.0 149.7 jit_solution(869015864135195048)
XLA Ops:
  0.0 148.7 %shard_map.100 = bf16[320,2048]{1,0:T(8,128)(2,1)S(1)} custom-call(bf16[640,512]{1,0:T(8,128)(2,1)} %q_hbm.1, bf16[640,128]{1,0:T(8,128)(2,1)} %k_hbm.1, bf16[640,128]{1,0:T(8,128)(2,1)} %v_hbm.1, s32[640]{0:T(1024)} %docs_hbm.1, f32[8]{0:T(128)} %sinks_hbm.1, bf16[1024,2048]{1,0:T(8,128)(2,1)} %outw_hbm.1, bf16[320,2048]{1,0:T(8,128)(2,1)} %res_hbm.1, ...), custom_call_target="tpu_custom_call" | custom-call | tf_op jit(solution)/shard_map/pallas_call | solution.py:671
  148.7 1.1 copy.12

commit v5 on v4

--- a/solution.py
+++ b/solution.py
@@ -161,7 +161,7 @@
     up_all, down_all, rows_all, hid_all, outw, res, mixed, q_ref, k_ref, v_ref, docs, docs_prev, docs_flat, sinks, gain_ref,
     k_wide, v_wide, att, oth, psend, precv, own_sum,
     load_sem, halo_send, halo_recv, xs_sem, xr_sem, z_send, z_recv, d_send, d_recv, y_sem,
-    g_send, g_recv, p_send, p_recv, own_sem,
+    g_send, g_recv, p_send, p_recv, own_sem, tail_sem,
 ):
     sp, y = lax.axis_index("sp"), lax.axis_index("tp")
     n_x, n_y = 2, 2
@@ -236,8 +236,8 @@
         slot = 0 if phase == 0 else 1 + zb * n_x + b
         return remote(ref, ref, d_send.at[phase], d_recv.at[slot], c_peer)
 
-    def to_core_all(phase):
-        ref = up_all.at[pl.ds(0, model // 2), :] if phase == 0 else down_all.at[pl.ds(0, n_z)]
+    def to_core_all(phase, less=0):
+        ref = up_all.at[pl.ds(0, (2 * n_z - less) * blk), :]
         return remote(ref, ref, d_send.at[phase], d_recv.at[0], c_peer)
 
     def goes_up(zb):
@@ -621,13 +621,65 @@
 
     lax.fori_loop(0, n_whole, down_step, 0)
 
+    at_end = jnp.logical_or(z == 0, z == n_z - 1)
+    z_last, _, x_last = place(n_items - 1)
+    last_slot = 1 + z_last * n_x + 1
+
+    def tail_half(part, send, recv, dev):
+        ref = part_of(block(1, z_last, x_last, 0), part)
+        return remote(ref, ref, send, recv, dev)
+
+    def tail_first():
+        tail_half(0, tail_sem.at[0], z_recv.at[1, z_last, 1], c_peer).wait_recv()
+        tail_half(0, tail_sem.at[0], d_recv.at[last_slot], c_peer).start()
+
+    def tail_second():
+        tail_half(1, tail_sem.at[0], tail_sem.at[1], c_peer).wait_recv()
+        tail_half(1, tail_sem.at[0], tail_sem.at[1], c_peer).start()
+        tail_half(0, tail_sem.at[0], d_recv.at[last_slot], c_peer).wait_recv()
+
+    def tail_forward():
+        to_up(1, z_last, 1, x_last).wait_recv()
+        for outer, towards in ((n_z - 1, 1), (0, -1)):
+            @pl.when(jnp.logical_and(z + towards == outer, (z_last - z) * towards < 0))
+            def _():
+                tail_half(0, z_send.at[1], z_recv.at[1, z_last, 1], at(z + towards, x, y, 0)).start()
+                tail_half(1, z_send.at[1], tail_sem.at[1], at(z + towards, x, y, 1)).start()
+
+        to_core(1, z_last, 1, x_last).start()
+
     def last_step(t, carry):
         for h in (1, 0):
-            @pl.when(c == h)
+            halved = jnp.logical_and(t == n_items - 1, at_end)
+            if h == 1:
+                @pl.when(jnp.logical_and(halved, c == 0))
+                def _():
+                    tail_first()
+
+                own, other = c == 1, c == 0
+            else:
+                final = jnp.logical_and(t == n_items - 1, jnp.logical_not(at_end))
+
+                @pl.when(jnp.logical_and(halved, c == 0))
+                def _():
+                    tail_half(1, tail_sem.at[0], tail_sem.at[1], c_peer).wait_recv()
+
+                @pl.when(jnp.logical_and(halved, c == 1))
+                def _():
+                    tail_second()
+
+                @pl.when(jnp.logical_and(final, c == 0))
+                def _():
+                    tail_forward()
+
+                own = jnp.logical_and(c == 0, t < n_items - 1)
+                other = jnp.logical_and(c == 1, jnp.logical_not(halved))
+
+            @pl.when(own)
             def _():
                 arrive(1, t)
 
-            @pl.when(c != h)
+            @pl.when(other)
             def _():
                 zb, b, xb = place(t)
                 to_core(1, zb, b, xb).wait_recv()
@@ -646,8 +698,19 @@
     given = rows_all.at[pl.ds(0, 3 * rows), :]
     remote(given, given, g_send.at[0], g_recv.at[0], x_peer).wait_send()
     line_sent(1)
-    for phase in range(2):
-        to_core_all(phase).wait_send()
+    to_core_all(0).wait_send()
+
+    @pl.when(jnp.logical_or(jnp.logical_not(at_end), c == 1))
+    def _():
+        to_core_all(1).wait_send()
+
+    @pl.when(jnp.logical_and(at_end, c == 0))
+    def _():
+        to_core_all(1, 1).wait_send()
+
+    @pl.when(at_end)
+    def _():
+        tail_half(0, tail_sem.at[0], tail_sem.at[1], c_peer).wait_send()
 
     for t in range(n_whole - 1, n_items):
         for h in (None,) if t < n_whole else (1, 0):
@@ -698,7 +761,7 @@
             pltpu.VMEM((pairs, rows, 2 * blk), f32),
             dma((8,)), dma((3,)), dma((3,)), dma((2,)), dma((2, 2)), dma((2,)), dma((2, n_z, 2)),
             dma((2,)), dma((1 + 2 * n_z,)), dma((2,)), dma((1,)), dma((8,)),
-            dma((1,)), dma((pairs + 2,)), dma((2,)),
+            dma((1,)), dma((pairs + 2,)), dma((2,)), dma((2,)),
         ],
         compiler_params=pltpu.CompilerParams(collective_id=0, has_side_effects=True, vmem_limit_bytes=60 << 20),
     )(

time: 151 us -> 151 us (level)
  no operation moved by 1% of the time
where the time goes in v5:
time: 151 us
  Pallas kernels  150 us (99%)
    pallas_call x1, Pallas kernels, kernel_body(): pl.pallas_call(functools.partial(layer_kernel, n_z), out_shape=pltpu.VMEM...  150 us

profile of v5, /device:TPU:0, one launch (start us, length us, event | category | flops | bytes accessed | tf_op | source)
XLA Modules:
  0.0 150.7 jit_solution(12933414952918074643)
XLA Ops:
  0.0 149.7 %shard_map.100 = bf16[320,2048]{1,0:T(8,128)(2,1)S(1)} custom-call(bf16[640,512]{1,0:T(8,128)(2,1)} %q_hbm.1, bf16[640,128]{1,0:T(8,128)(2,1)} %k_hbm.1, bf16[640,128]{1,0:T(8,128)(2,1)} %v_hbm.1, s32[640]{0:T(1024)} %docs_hbm.1, f32[8]{0:T(128)} %sinks_hbm.1, bf16[1024,2048]{1,0:T(8,128)(2,1)} %outw_hbm.1, bf16[320,2048]{1,0:T(8,128)(2,1)} %res_hbm.1, ...), custom_call_target="tpu_custom_call" | custom-call | tf_op jit(solution)/shard_map/pallas_call | solution.py:734
  149.7 1.1 copy.12
